TPU v7x, 128 devices: a whole 4x4x4 slice. The times are simulated.
128 devices in a mesh: sp: 16 (over z, y), tp: 8 (over x, core).
Axes of the slice: x: 4, y: 4, z: 4, core: 2. Of those that a mesh axis runs over, the one named last changes fastest.
Arguments:
- skip_stream_vector: bfloat16 [16384, 2048], P(('sp', 'tp')), may hold values from -6 to 6
- probe_preactivation: bfloat16 [16384, 1024], P('sp', 'tp'), may hold values from -6 to 6
- retention_preactivation: bfloat16 [16384, 1024], P('sp', 'tp'), may hold values from -4.5 to 4.5
- content_vector: bfloat16 [16384, 1024], P('sp', 'tp'), may hold values from -6 to 6
- emission_preactivation: bfloat16 [16384, 1024], P('sp', 'tp'), may hold values from -6 to 6
- retention_slack: float32 [1024], P('tp'), may hold values from 0 to 0.12
- surge_rate: float32 [16384, 1024], P('sp', 'tp'), may hold values from -1.2 to 0
- subspace_scaling_factor: float32 [1024], P('tp'), may hold values from 0.1 to 1.9
- emission_matrix: bfloat16 [1024, 2048], replicated, may hold values from -0.1875 to 0.1875
- mlp_scaling_factor: float32 [2048], replicated, may hold values from 0.1 to 1.9
- switch_matrix: bfloat16 [2048, 5632], P('sp', 'tp'), may hold values from -0.125 to 0.125
- expansion_matrix: bfloat16 [2048, 5632], P('sp', 'tp'), may hold values from -0.125 to 0.125
- contraction_matrix: bfloat16 [5632, 2048], P('tp', 'sp'), may hold values from -0.078125 to 0.078125
Outputs:
- stream_out: bfloat16 [16384, 2048], P(('sp', 'tp'))
All inputs are finite; a program needn't handle non-finite values.
Results may differ from a plain program's by a relative error of at most 0.017.
Values may be sent and summed in bfloat16 or wider, within the bound.
A program may use at most 128 MiB of HBM per device.

v0:
```python
import jax
import jax.numpy as jnp
from jax import lax
from jax.sharding import Mesh
from jax.sharding import PartitionSpec as P

HEAD_DIM = 128
BLOCK = 64
TP = ("tp_0", "tp_1")
SP_TP = ("sp", "tp_0", "tp_1")
EPSILON = 1e-06
TOP_PRECISION = lax.Precision.HIGHEST


def in_one_piece(arrays, axis, dim, along):
    both = jnp.concatenate(arrays, axis=along)
    whole, at, outs = (lax.all_gather(both, axis, axis=dim, tiled=True), 0, [])
    for a in arrays:
        outs.append(lax.slice_in_dim(whole, at, at + a.shape[along], axis=along))
        at += a.shape[along]
    return tuple(outs)


def from_everyone(value, axis):
    peers = lax.axis_size(axis)
    return lax.all_to_all(
        jnp.broadcast_to(value[None], (peers, *value.shape)), axis, 0, 0, tiled=True
    )


def all_in_one(value, axis):
    leaves = jax.tree.leaves(value)
    order = sorted(range(len(leaves)), key=lambda k: -leaves[k].size)
    width = (1, *leaves[order[0]].shape)[-1]
    lines = [
        jnp.pad(leaves[k].reshape(-1), (0, -leaves[k].size % width)).reshape(-1, width)
        for k in order
    ]
    both, at, found = (from_everyone(jnp.concatenate(lines), axis), 0, {})
    for k, line in zip(order, lines):
        piece = both[:, at : at + len(line)].reshape(len(both), -1)
        found[k] = piece[:, : leaves[k].size].reshape(-1, *leaves[k].shape)
        at += len(line)
    numbers = iter(range(len(leaves)))
    return jax.tree.map(lambda _: found[next(numbers)], value)


def joined_by_halves(pieces, combine):
    while len(jax.tree.leaves(pieces)[0]) > 1:
        pieces = jax.vmap(combine)(
            *(jax.tree.map(lambda part: part[side::2], pieces) for side in (0, 1))
        )
    return jax.tree.map(lambda part: part[0], pieces)


def carried_in(value, axis, combine, identity):
    peers, here = (lax.axis_size(axis), lax.axis_index(axis))
    passed = jnp.arange(peers) < here

    def kept(part, zero, own):
        part = jnp.where(
            passed.reshape(-1, *(1 for _ in own.shape)),
            part.astype(own.dtype),
            jnp.asarray(zero, own.dtype),
        )
        return part

    pieces = all_in_one(
        jax.tree.map(lambda part, kind: part.astype(kind), value, (jnp.bfloat16, jnp.bfloat16)),
        axis,
    )
    return joined_by_halves(jax.tree.map(kept, pieces, identity, value), combine)


def joined_along(tiles, dim):
    lengths = list(tiles.shape[1:])
    lengths[dim] *= tiles.shape[0]
    return jnp.moveaxis(tiles, 0, dim).reshape(lengths)


def gathered_by_axis(value, axes, dim):
    far, near = axes
    tiles = from_everyone(from_everyone(value, far), near)
    return joined_along(tiles.swapaxes(0, 1).reshape(-1, *value.shape), dim)


def in_blocks(value, dim, peers):
    lengths = value.shape
    tiles = value.reshape(*lengths[:dim], peers, lengths[dim] // peers, *lengths[dim + 1 :])
    return jnp.moveaxis(tiles, dim, 0)


def summed_on_arrival(value, axis, dim):
    tiles = in_blocks(value, dim, lax.axis_size(axis))
    arrived = lax.all_to_all(tiles, axis, split_axis=0, concat_axis=0, tiled=True)
    return arrived.astype(jnp.float32).sum(axis=0)


def sum_by_axis(value, axes, dim):
    far, near = axes
    own = summed_on_arrival(in_blocks(value, dim, lax.axis_size(far)), near, dim + 1)
    return jnp.sum(
        lax.all_to_all(own.astype(jnp.bfloat16), far, 0, 0, tiled=True).astype(jnp.float32), axis=0
    )


def block_step(carry, inputs):
    memory_state, offsets = carry
    query_block, input_gate_block, value_block, log_blk = inputs
    cumulative_decay = jnp.cumsum(log_blk, axis=1)
    length = log_blk.shape[1]
    carried_share = jnp.einsum(
        "eia,eax->eix",
        query_block * jnp.exp(cumulative_decay),
        memory_state,
        precision=TOP_PRECISION,
    )
    middle = cumulative_decay[:, length // 2, :][:, None, :]
    left_side = query_block * jnp.exp(cumulative_decay - middle)
    right_side = input_gate_block * jnp.exp(middle - cumulative_decay)
    causal = (jnp.arange(length)[:, None] >= jnp.arange(length)[None, :])[None, :, :]
    scores = jnp.einsum("htk,hsk->hts", left_side, right_side, precision=TOP_PRECISION)
    scores = jnp.where(causal, scores, 0.0)
    outputs = carried_share + jnp.einsum(
        "hts,hsv->htv", scores, value_block, precision=TOP_PRECISION
    )
    closing_log_decay = cumulative_decay[:, -1, :]
    updated_memory_state = jnp.exp(closing_log_decay)[:, :, None] * memory_state + jnp.einsum(
        "qnj,qnl->qjl",
        input_gate_block * jnp.exp(closing_log_decay[:, None, :] - cumulative_decay),
        value_block,
        precision=TOP_PRECISION,
    )
    return (
        (updated_memory_state, offsets + closing_log_decay),
        (outputs, cumulative_decay + offsets[:, None, :]),
    )


def split_blocks(values, heads_here):
    count = values.shape[0]
    return values.reshape(count // BLOCK, BLOCK, heads_here, HEAD_DIM).transpose(0, 2, 1, 3)


def admission_source_matrix(
    probe_preactivation, retention_preactivation, content_vector, retention_slack, surge_rate
):
    query_act = jax.nn.silu(probe_preactivation.astype(jnp.float32))
    admission_factor = retention_slack[None, :] * jax.nn.sigmoid(
        -retention_preactivation.astype(jnp.float32)
    )
    retention_logarithm = jnp.log1p(-admission_factor) + surge_rate
    return (query_act, admission_factor, content_vector.astype(jnp.float32), retention_logarithm)


def head_output(outputs, subspace_scaling_factor, emission_preactivation):
    count, heads_here = (outputs.shape[0], outputs.shape[1])
    squares = jnp.mean(outputs * outputs, axis=-1, keepdims=True)
    scaled = (
        outputs
        * lax.rsqrt(squares + EPSILON)
        * subspace_scaling_factor.reshape(heads_here, HEAD_DIM)
    )
    scaled = scaled.reshape(count, heads_here * HEAD_DIM)
    return (scaled * jax.nn.silu(emission_preactivation.astype(jnp.float32))).astype(jnp.bfloat16)


def row_norm(stream, mlp_scaling_factor):
    streamf = stream.astype(jnp.float32)
    squares = jnp.mean(streamf * streamf, axis=-1, keepdims=True)
    return (streamf * lax.rsqrt(squares + EPSILON) * mlp_scaling_factor).astype(jnp.bfloat16)


def chain(earlier, later):
    return (earlier[0] * later[0], later[0][:, :, None] * earlier[1] + later[1])


def on_device(
    skip_stream_vector,
    probe_preactivation,
    retention_preactivation,
    content_vector,
    emission_preactivation,
    retention_slack,
    surge_rate,
    subspace_scaling_factor,
    emission_matrix,
    mlp_scaling_factor,
    switch_matrix,
    expansion_matrix,
    contraction_matrix,
):
    gate_whole, up_whole = in_one_piece((switch_matrix, expansion_matrix), "sp", 0, 1)
    down_whole = lax.all_gather(contraction_matrix, "sp", axis=1, tiled=True)
    heads_here = probe_preactivation.shape[1] // HEAD_DIM
    tok_rows = probe_preactivation.shape[0]
    arranged_sources = admission_source_matrix(
        probe_preactivation, retention_preactivation, content_vector, retention_slack, surge_rate
    )
    block_list = tuple((split_blocks(item, heads_here) for item in arranged_sources))
    start_carry = (
        jnp.zeros((heads_here, HEAD_DIM, HEAD_DIM), jnp.float32),
        jnp.zeros((heads_here, HEAD_DIM), jnp.float32),
    )
    (memory_state, offsets), (outputs, cumulative_log_decay) = lax.scan(
        block_step, start_carry, block_list
    )
    incoming_state = carried_in(
        (jnp.exp(offsets), memory_state),
        "sp",
        chain,
        (jnp.ones_like(offsets), jnp.zeros_like(memory_state)),
    )
    outputs = outputs + jnp.einsum(
        "jmxo,mos->jmxs",
        block_list[0] * jnp.exp(cumulative_log_decay),
        incoming_state[1],
        precision=TOP_PRECISION,
    )
    outputs = outputs.transpose(0, 2, 1, 3).reshape(tok_rows, heads_here, HEAD_DIM)
    mixed = head_output(outputs, subspace_scaling_factor, emission_preactivation)
    regrouped = lax.all_to_all(mixed, TP, split_axis=0, concat_axis=1, tiled=True)
    projected = jnp.dot(regrouped, emission_matrix, preferred_element_type=jnp.float32)
    stream = (skip_stream_vector.astype(jnp.float32) + projected).astype(jnp.bfloat16)
    normed = row_norm(stream, mlp_scaling_factor)
    all_rows = gathered_by_axis(normed, ("tp_0", "tp_1"), 0)
    gate_proj = jnp.dot(all_rows, gate_whole, preferred_element_type=jnp.float32)
    up_proj = jnp.dot(all_rows, up_whole, preferred_element_type=jnp.float32)
    hidden = (jax.nn.silu(gate_proj) * up_proj).astype(jnp.bfloat16)
    partial_sum = jnp.dot(hidden, down_whole, preferred_element_type=jnp.float32)
    summed = sum_by_axis(partial_sum.astype(jnp.bfloat16), ("tp_0", "tp_1"), 0)
    return (stream.astype(jnp.float32) + summed).astype(jnp.bfloat16)


def solution(mesh):
    split = Mesh(mesh.devices.reshape(mesh.shape["sp"], 4, 2), ("sp", "tp_0", "tp_1"))
    return jax.shard_map(
        on_device,
        mesh=split,
        in_specs=(
            P(SP_TP, None),
            P("sp", TP),
            P("sp", TP),
            P("sp", TP),
            P("sp", TP),
            P(TP),
            P("sp", TP),
            P(TP),
            P(),
            P(),
            P("sp", TP),
            P("sp", TP),
            P(TP, "sp"),
        ),
        out_specs=P(SP_TP, None),
        check_vma=False,
    )
```

profile of v0, /device:TPU:0, one launch (start us, length us, event | category | flops | bytes accessed | tf_op | source)
XLA Modules:
  0.0 193.7 jit_solution(10395686392634396452)
XLA Ops:
  6.5 1.8 pad_maximum_fusion
  8.4 1.1 convert_multiply_fusion.1
  9.5 1.0 convert.2
  10.5 1.5 divide_multiply_fusion
  12.0 17.0 %while.17 = (s32[]{:T(128)}, f32[1,128,128]{2,1,0:T(8,128)S(1)}, f32[1,128]{1,0:T(1,128)S(1)}, f32[16,1,64,128]{3,2,1,0:T(8,128)S(1)}, f32[16,1,64,128]{3,2,1,0:...) while((s32[]{:T(128)}, f32[1,128,128]{2,1,0:T(8,128)S(1)}, ...), condition=%wide.region_2.3_spmd.clone, body=%wide.region_0.2_spmd.clone.sunk | while | flops 38412544 | bytes 879768 | solution.py:205
  12.5 0.3 fusion.99
  13.6 0.3 fusion.99
  14.7 0.3 fusion.99
  15.7 0.3 fusion.99
  17.8 0.3 fusion.99
  18.9 0.3 fusion.99
  21.0 0.3 fusion.99
  29.0 0.9 broadcast_in_dim.48
  29.9 8.2 %all-to-all-start = ((bf16[16,129,128]{2,1,0:T(8,128)(2,1)}), bf16[16,129,128]{2,1,0:T(8,128)(2,1)S(1)}, u32[]{:S(2)}, u32[]{:S(2)}) async-start(bf16[16,129,128]{2,1,0:T(8,128)(2,1)} %broadcast_in_dim.48), calls=%async_computation | async-start | bytes 1114112 | tf_op jit(solution)/shard_map/all_to_all | solution.py:26
  38.1 0.7 all-gather.5.cloned.1.call-update
  38.9 11.2 %all-to-all-done = bf16[16,129,128]{2,1,0:T(8,128)(2,1)S(1)} async-done(((bf16[16,129,128]{2,1,0:T(8,128)(2,1)}), bf16[16,129,128]{2,1,0:T(8,128)(2,1)S(1)}, u32[]{:S(2)}, u32[]{:S(2)}) %all-to-all-start) | async-done | bytes 528416 | tf_op jit(solution)/shard_map/all_to_all | solution.py:26
  50.8 0.7 multiply_reduce_fusion.1
  51.9 11.6 %all_to_all.44 = bf16[8,128,128]{2,1,0:T(8,128)(2,1)S(1)} all-to-all(bf16[8,128,128]{2,1,0:T(8,128)(2,1)S(1)} %bitcast.185), channel_id=1, replica_groups=mesh['sp'=16,'tp_0'=4,'tp_1'=2] {'tp_0','tp_1'}, dimensions={0} | all-to-all | bytes 524288 | tf_op jit(solution)/shard_map/all_to_all | solution.py:222
  63.7 3.0 %multiply_reduce_fusion = (f32[128]{0:T(128)S(1)}, f32[128,2048]{1,0:T(8,128)S(1)}) fusion(bf16[128,1024]{0,1:T(8,128)(2,1)S(1)} %bitcast.183, bf16[1024,2048]{1,0:T(8,128)(2,1)} %param.23, bf16[128,2048]{1,0:T(8,128)(2,1)S(1)} %copy-done), kind=kOutput, calls=%fused_computation.66 | convolution fusion | flops 538443648 | bytes 6029824 | tf_op jit(solution)/shard_map/dot_general | solution.py:223
  67.1 28.8 %all_to_all.45 = bf16[4,128,2048]{2,1,0:T(8,128)(2,1)S(1)} all-to-all(bf16[4,128,2048]{2,1,0:T(8,128)(2,1)S(1)} %broadcast_in_dim.74), channel_id=1, replica_groups=mesh['sp'=16,'tp_0'=4,'tp_1'=2] {'tp_0'}, dimensions={0} | all-to-all | bytes 4194304 | tf_op jit(solution)/shard_map/all_to_all | solution.py:26
  95.9 0.5 broadcast_in_dim.75
  96.5 7.1 %all_to_all.46 = bf16[2,4,128,2048]{3,2,1,0:T(8,128)(2,1)S(1)} all-to-all(bf16[2,4,128,2048]{3,2,1,0:T(8,128)(2,1)S(1)} %broadcast_in_dim.75), channel_id=1, replica_groups=mesh['sp'=16,'tp_0'=4,'tp_1'=2] {'tp_1'}, dimensions={0} | all-to-all | bytes 8388608 | tf_op jit(solution)/shard_map/all_to_all | solution.py:26
  103.6 2.3 %copy.36 = bf16[2,4,128,2048]{3,2,0,1:T(8,128)(2,1)} copy(bf16[2,4,128,2048]{3,2,1,0:T(8,128)(2,1)S(1)} %all_to_all.46) | data formatting | bytes 8388608 | tf_op jit(solution)/shard_map/all_to_all | solution.py:26
  105.9 7.9 %fusion.43 = f32[1024,704]{0,1:T(8,128)} fusion(bf16[1024,2048]{1,0:T(8,128)(2,1)} %bitcast.178, bf16[2048,1408]{0,1:T(8,128)(2,1)} %all-gather.3.cloned.1.call-done), kind=kOutput, calls=%fused_computation.56 | convolution fusion | flops 2952790016 | bytes 9961472 | tf_op jit(solution)/shard_map/dot_general | solution.py:227
  113.8 14.8 %all-gather.5.cloned.1.call-done = bf16[704,2048]{1,0:T(8,128)(2,1)} async-done(((bf16[704,128]{1,0:T(8,128)(2,1)}), bf16[704,2048]{1,0:T(8,128)(2,1)}) %all-gather.5.cloned.1.call-update) | async-done | bytes 2883600 | tf_op jit(solution)/shard_map/all_gather | solution.py:194
  128.6 12.1 %convolution_convert_fusion = bf16[1024,2048]{1,0:T(8,128)(2,1)} fusion(bf16[704,2048]{1,0:T(8,128)(2,1)} %all-gather.5.cloned.1.call-done, f32[1024,704]{0,1:T(8,128)} %fusion.43, bf16[1024,2048]{1,0:T(8,128)(2,1)} %bitcast.179, bf16[2048,1408]{0,1:T(8,128)(2,1)} %all-gather.3.cloned.1.call-done), kind=kOutput, calls=%fused_computation.53 | convolution fusion | flops 5912002560 | bytes 17039360 | tf_op jit(solution)/shard_map/dot_general | solution.py:230
  140.7 2.5 %copy.39 = bf16[4,2,128,2048]{3,2,0,1:T(8,128)(2,1)S(1)} copy(bf16[4,2,128,2048]{3,2,1,0:T(8,128)(2,1)} %bitcast.180) | data formatting | bytes 8388608 | tf_op jit(solution)/shard_map/reshape;reshape | solution.py:89
  143.2 8.2 %all_to_all.47 = bf16[2,4,128,2048]{3,2,1,0:T(8,128)(2,1)} all-to-all(bf16[2,4,128,2048]{3,2,1,0:T(8,128)(2,1)S(1)} %bitcast.177), channel_id=1, replica_groups=mesh['sp'=16,'tp_0'=4,'tp_1'=2] {'tp_1'}, dimensions={0} | all-to-all | bytes 8388608 | tf_op jit(solution)/shard_map/all_to_all | solution.py:95
  151.3 3.5 %reduce_sum.41 = bf16[4,128,2048]{2,1,0:T(8,128)(2,1)S(1)} reduce(bf16[2,4,128,2048]{3,2,1,0:T(8,128)(2,1)} %all_to_all.47, bf16[]{:T(256)} %constant.49.clone.1), dimensions={0}, to_apply=%region_5.6 | reduce | flops 1048576 | bytes 6291458 | tf_op jit(solution)/shard_map/reduce_sum | solution.py:96
  154.9 30.7 %all_to_all.48 = bf16[4,128,2048]{2,1,0:T(8,128)(2,1)S(1)} all-to-all(bf16[4,128,2048]{2,1,0:T(8,128)(2,1)S(1)} %reduce_sum.41), channel_id=1, replica_groups=mesh['sp'=16,'tp_0'=4,'tp_1'=2] {'tp_0'}, dimensions={0} | all-to-all | bytes 4194304 | tf_op jit(solution)/shard_map/all_to_all | solution.py:103
  185.6 0.4 convert_reduce_fusion
  186.0 0.9 add_convert_fusion
  (189 shorter events, 15.5 us)
Async XLA Ops:
  6.5 99.4 %all-gather.3.cloned.1.call-start = ((), (), s32[]{:S(2)}) async-start(), calls=%async_computation.6 | async-start | bytes 6127616 | tf_op jit(solution)/shard_map/all_gather | solution.py:17
  29.9 20.2 %all-to-all-start = ((bf16[16,129,128]{2,1,0:T(8,128)(2,1)}), bf16[16,129,128]{2,1,0:T(8,128)(2,1)S(1)}, u32[]{:S(2)}, u32[]{:S(2)}) async-start(bf16[16,129,128]{2,1,0:T(8,128)(2,1)} %broadcast_in_dim.48), calls=%async_computation | async-start | bytes 1114112 | tf_op jit(solution)/shard_map/all_to_all | solution.py:26
  38.1 90.5 %all-gather.5.cloned.1.call-start = ((), (), s32[]{:S(2)}) async-start(), calls=%async_computation.7 | async-start | bytes 3063808 | tf_op jit(solution)/shard_map/all_gather | solution.py:194
  50.3 1.3 copy-start.1
  50.3 1.3 copy-start.3
  50.6 13.1 %copy-start = (bf16[128,2048]{1,0:T(8,128)(2,1)S(1)}, bf16[128,2048]{1,0:T(8,128)(2,1)}, u32[]{:S(2)}) copy-start(bf16[128,2048]{1,0:T(8,128)(2,1)} %param.15) | copy-start | bytes 1572868
  63.7 3.0 %copy-start.2 = (f32[2048]{0:T(1024)S(1)}, f32[2048]{0:T(1024)}, u32[]{:S(2)}) copy-start(f32[2048]{0:T(1024)} %param.24) | copy-start | bytes 24580
Sparse Core Ops, SparseCore 0:
  9.4 66.9 all-gather.2
  78.6 49.9 all-gather.4
where the time goes:
time: 194 us
  blocking collectives  86.3 us (44%)
  matrix products  37.4 us (19%)
  waiting for transfers between devices  26.8 us (14%)
  between operations  13.7 us (7%)
  other arithmetic  13.2 us (7%)
  starting transfers between devices  8.21 us (4%)
  local copies, waits for them, and re-layouts  7.13 us (4%)
    all_to_all x2, blocking collectives, from_everyone(): lax.all_to_all(jnp.broadcast_to(value[None], (peers, *value.shape)), axis...  35.9 us
    all_to_all x1, blocking collectives, sum_by_axis(): lax.all_to_all(own.astype(jnp.bfloat16), far, 0, 0, tiled=True)  30.7 us
    all_gather x1, waiting for transfers between devices, on_device(): down_whole = lax.all_gather(contraction_matrix, 'sp', axis=1, tiled=True)  14.8 us
    dot_general x1, matrix products, on_device(): jnp.dot(hidden, down_whole, preferred_element_type=jnp.float32)  12.1 us
    all_to_all x1, blocking collectives, on_device(): lax.all_to_all(mixed, TP, split_axis=0, concat_axis=1, tiled=True)  11.6 us
    all_to_all x1, waiting for transfers between devices, from_everyone(): lax.all_to_all(jnp.broadcast_to(value[None], (peers, *value.shape)), axis...  11.2 us
    all_to_all x1, blocking collectives, summed_on_arrival(): lax.all_to_all(tiles, axis, split_axis=0, concat_axis=0, tiled=True)  8.18 us
    all_to_all x1, starting transfers between devices, from_everyone(): lax.all_to_all(jnp.broadcast_to(value[None], (peers, *value.shape)), axis...  8.16 us
  transfers between devices with their start and end apart: 3, of which 2 were waited for; matrix products, arithmetic and copies ran while one was open for 19% of the time, Pallas kernels for 0%

commit v1 on v0

--- a/solution.py
+++ b/solution.py
@@ -10,6 +10,12 @@
 SP_TP = ("sp", "tp_0", "tp_1")
 EPSILON = 1e-06
 TOP_PRECISION = lax.Precision.HIGHEST
+
+
+def gather_from_all(x, axis, dim):
+    count = lax.axis_size(axis)
+    repeats = [count if d == dim else 1 for d in range(x.ndim)]
+    return lax.all_to_all(jnp.tile(x, repeats), axis, split_axis=dim, concat_axis=dim, tiled=True)
 
 
 def in_one_piece(arrays, axis, dim, along):
@@ -191,7 +197,7 @@
     contraction_matrix,
 ):
     gate_whole, up_whole = in_one_piece((switch_matrix, expansion_matrix), "sp", 0, 1)
-    down_whole = lax.all_gather(contraction_matrix, "sp", axis=1, tiled=True)
+    down_whole = gather_from_all(contraction_matrix, "sp", 1)
     heads_here = probe_preactivation.shape[1] // HEAD_DIM
     tok_rows = probe_preactivation.shape[0]
     arranged_sources = admission_source_matrix(

time: 194 us -> 221 us (1.14)
  waiting for transfers between devices: 26.8 us -> 44.4 us
  local copies, waits for them, and re-layouts: 7.13 us -> 11.8 us
  starting transfers between devices: 8.21 us -> 12.8 us
    all_to_all x0 -> x1, waiting for transfers between devices: none -> 32.4 us  [gather_from_all(): lax.all_to_all(jnp.tile(x, repeats), axis, split_axis=dim, concat_axis=di...]
    all_gather x1 -> x0, waiting for transfers between devices: 14.8 us -> none  [on_device(): down_whole = lax.all_gather(contraction_matrix, 'sp', axis=1, tiled=True)]
    all_to_all x0 -> x1, starting transfers between devices: none -> 4.64 us  [gather_from_all(): lax.all_to_all(jnp.tile(x, repeats), axis, split_axis=dim, concat_axis=di...]
    all_to_all x1, local copies, waits for them, and re-layouts: 2.33 us -> 4.8 us  [from_everyone(): lax.all_to_all(jnp.broadcast_to(value[None], (peers, *value.shape)), axis...]
where the time goes in v1:
time: 221 us; the launch traced here: 220 us
  blocking collectives  86.2 us (39%)
  waiting for transfers between devices  44.4 us (20%)
  matrix products  37.4 us (17%)
  between operations  13.7 us (6%)
  other arithmetic  13.1 us (6%)
  starting transfers between devices  12.8 us (6%)
  local copies, waits for them, and re-layouts  11.8 us (5%)
    all_to_all x2, blocking collectives, from_everyone(): lax.all_to_all(jnp.broadcast_to(value[None], (peers, *value.shape)), axis...  37 us
    all_to_all x1, waiting for transfers between devices, gather_from_all(): lax.all_to_all(jnp.tile(x, repeats), axis, split_axis=dim, concat_axis=di...  32.4 us
    all_to_all x1, blocking collectives, sum_by_axis(): lax.all_to_all(own.astype(jnp.bfloat16), far, 0, 0, tiled=True)  29.4 us
    dot_general x1, matrix products, on_device(): jnp.dot(hidden, down_whole, preferred_element_type=jnp.float32)  12 us
    all_to_all x1, waiting for transfers between devices, from_everyone(): lax.all_to_all(jnp.broadcast_to(value[None], (peers, *value.shape)), axis...  12 us
    all_to_all x1, blocking collectives, on_device(): lax.all_to_all(mixed, TP, split_axis=0, concat_axis=1, tiled=True)  11.6 us
    all_to_all x1, blocking collectives, summed_on_arrival(): lax.all_to_all(tiles, axis, split_axis=0, concat_axis=0, tiled=True)  8.18 us
    all_to_all x1, starting transfers between devices, from_everyone(): lax.all_to_all(jnp.broadcast_to(value[None], (peers, *value.shape)), axis...  8.16 us
  transfers between devices with their start and end apart: 3, of which 2 were waited for; matrix products, arithmetic and copies ran while one was open for 19% of the time, Pallas kernels for 0%

profile of v1, /device:TPU:0, one launch (start us, length us, event | category | flops | bytes accessed | tf_op | source)
XLA Modules:
  0.0 220.4 jit_solution(11975222686143445894)
XLA Ops:
  6.5 1.8 pad_maximum_fusion
  8.4 1.1 convert_multiply_fusion.1
  9.5 1.0 convert.2
  10.5 1.4 divide_multiply_fusion
  11.9 17.0 %while.17 = (s32[]{:T(128)}, f32[1,128,128]{2,1,0:T(8,128)S(1)}, f32[1,128]{1,0:T(1,128)S(1)}, f32[16,1,64,128]{3,2,1,0:T(8,128)S(1)}, f32[16,1,64,128]{3,2,1,0:...) while((s32[]{:T(128)}, f32[1,128,128]{2,1,0:T(8,128)S(1)}, ...), condition=%wide.region_2.3_spmd.clone, body=%wide.region_0.2_spmd.clone.sunk | while | flops 38412544 | bytes 879768 | solution.py:211
  13.5 0.3 fusion.101
  14.6 0.3 fusion.101
  15.7 0.3 fusion.101
  16.7 0.3 fusion.101
  17.8 0.3 fusion.101
  18.9 0.3 fusion.101
  29.0 0.9 broadcast_in_dim.48
  29.9 8.2 %all-to-all-start = ((bf16[16,129,128]{2,1,0:T(8,128)(2,1)}), bf16[16,129,128]{2,1,0:T(8,128)(2,1)S(1)}, u32[]{:S(2)}, u32[]{:S(2)}) async-start(bf16[16,129,128]{2,1,0:T(8,128)(2,1)} %broadcast_in_dim.48), calls=%async_computation | async-start | bytes 1114112 | tf_op jit(solution)/shard_map/all_to_all | solution.py:32
  38.0 12.0 %all-to-all-done = bf16[16,129,128]{2,1,0:T(8,128)(2,1)S(1)} async-done(((bf16[16,129,128]{2,1,0:T(8,128)(2,1)}), bf16[16,129,128]{2,1,0:T(8,128)(2,1)S(1)}, u32[]{:S(2)}, u32[]{:S(2)}) %all-to-all-start) | async-done | bytes 528416 | tf_op jit(solution)/shard_map/all_to_all | solution.py:32
  50.8 0.7 multiply_reduce_fusion.1
  51.8 11.6 %all_to_all.53 = bf16[8,128,128]{2,1,0:T(8,128)(2,1)S(1)} all-to-all(bf16[8,128,128]{2,1,0:T(8,128)(2,1)S(1)} %bitcast.191), channel_id=1, replica_groups=mesh['sp'=16,'tp_0'=4,'tp_1'=2] {'tp_0','tp_1'}, dimensions={0} | all-to-all | bytes 524288 | tf_op jit(solution)/shard_map/all_to_all | solution.py:228
  63.6 3.0 %multiply_reduce_fusion = (f32[128]{0:T(128)S(1)}, f32[128,2048]{1,0:T(8,128)S(1)}) fusion(bf16[128,1024]{0,1:T(8,128)(2,1)S(1)} %bitcast.189, bf16[1024,2048]{1,0:T(8,128)(2,1)} %param.23, bf16[128,2048]{1,0:T(8,128)(2,1)S(1)} %copy-done), kind=kOutput, calls=%fused_computation.68 | convolution fusion | flops 538443648 | bytes 6029824 | tf_op jit(solution)/shard_map/dot_general | solution.py:229
  67.1 28.8 %all_to_all.54 = bf16[4,128,2048]{2,1,0:T(8,128)(2,1)S(1)} all-to-all(bf16[4,128,2048]{2,1,0:T(8,128)(2,1)S(1)} %broadcast_in_dim.74), channel_id=1, replica_groups=mesh['sp'=16,'tp_0'=4,'tp_1'=2] {'tp_0'}, dimensions={0} | all-to-all | bytes 4194304 | tf_op jit(solution)/shard_map/all_to_all | solution.py:32
  95.9 0.5 broadcast_in_dim.75
  96.4 8.3 %all_to_all.55 = bf16[2,4,128,2048]{3,2,1,0:T(8,128)(2,1)} all-to-all(bf16[2,4,128,2048]{3,2,1,0:T(8,128)(2,1)S(1)} %broadcast_in_dim.75), channel_id=1, replica_groups=mesh['sp'=16,'tp_0'=4,'tp_1'=2] {'tp_1'}, dimensions={0} | all-to-all | bytes 8388608 | tf_op jit(solution)/shard_map/all_to_all | solution.py:32
  104.7 2.2 tile.2
  106.8 4.6 %all-to-all-start.4 = ((bf16[704,16,128]{2,0,1:T(8,128)(2,1)}), bf16[704,16,128]{2,0,1:T(8,128)(2,1)}, u32[]{:S(2)}, u32[]{:S(2)}) async-start(bf16[704,16,128]{2,0,1:T(8,128)(2,1)} %tile.2), calls=%async_computation.4 | async-start | bytes 5767168 | tf_op jit(solution)/shard_map/all_to_all | solution.py:18
  111.5 4.8 %copy.45 = bf16[2,4,128,2048]{3,2,0,1:T(8,128)(2,1)} copy(bf16[2,4,128,2048]{3,2,1,0:T(8,128)(2,1)} %all_to_all.55) | data formatting | bytes 8388608 | tf_op jit(solution)/shard_map/all_to_all | solution.py:32
  116.3 7.8 %fusion.45 = f32[1024,704]{0,1:T(8,128)} fusion(bf16[1024,2048]{1,0:T(8,128)(2,1)} %bitcast.184, bf16[2048,1408]{0,1:T(8,128)(2,1)} %all-gather.2.cloned.1.call-done), kind=kOutput, calls=%fused_computation.58 | convolution fusion | flops 2952790016 | bytes 9961472 | tf_op jit(solution)/shard_map/dot_general | solution.py:233
  124.1 32.4 %all-to-all-done.4 = bf16[704,16,128]{2,0,1:T(8,128)(2,1)} async-done(((bf16[704,16,128]{2,0,1:T(8,128)(2,1)}), bf16[704,16,128]{2,0,1:T(8,128)(2,1)}, u32[]{:S(2)}, u32[]{:S(2)}) %all-to-all-start.4) | async-done | bytes 2883616 | tf_op jit(solution)/shard_map/all_to_all | solution.py:18
  156.6 12.0 %convolution_convert_fusion = bf16[1024,2048]{1,0:T(8,128)(2,1)} fusion(f32[1024,704]{0,1:T(8,128)} %fusion.45, bf16[1024,2048]{1,0:T(8,128)(2,1)} %bitcast.185, bf16[2048,1408]{0,1:T(8,128)(2,1)} %all-gather.2.cloned.1.call-done, bf16[704,16,128]{2,0,1:T(8,128)(2,1)} %all-to-all-done.4), kind=kOutput, calls=%fused_computation.53 | convolution fusion | flops 5912002560 | bytes 17039360 | tf_op jit(solution)/shard_map/dot_general | solution.py:236
  168.6 2.5 %copy.54 = bf16[4,2,128,2048]{3,2,0,1:T(8,128)(2,1)S(1)} copy(bf16[4,2,128,2048]{3,2,1,0:T(8,128)(2,1)} %bitcast.186) | data formatting | bytes 8388608 | tf_op jit(solution)/shard_map/reshape;reshape | solution.py:95
  171.1 8.2 %all_to_all.56 = bf16[2,4,128,2048]{3,2,1,0:T(8,128)(2,1)} all-to-all(bf16[2,4,128,2048]{3,2,1,0:T(8,128)(2,1)S(1)} %bitcast.183), channel_id=1, replica_groups=mesh['sp'=16,'tp_0'=4,'tp_1'=2] {'tp_1'}, dimensions={0} | all-to-all | bytes 8388608 | tf_op jit(solution)/shard_map/all_to_all | solution.py:101
  179.3 3.5 %reduce_sum.41 = bf16[4,128,2048]{2,1,0:T(8,128)(2,1)S(1)} reduce(bf16[2,4,128,2048]{3,2,1,0:T(8,128)(2,1)} %all_to_all.56, bf16[]{:T(256)} %constant.49.clone.1), dimensions={0}, to_apply=%region_5.6 | reduce | flops 1048576 | bytes 6291458 | tf_op jit(solution)/shard_map/reduce_sum | solution.py:102
  182.8 29.4 %all_to_all.57 = bf16[4,128,2048]{2,1,0:T(8,128)(2,1)S(1)} all-to-all(bf16[4,128,2048]{2,1,0:T(8,128)(2,1)S(1)} %reduce_sum.41), channel_id=1, replica_groups=mesh['sp'=16,'tp_0'=4,'tp_1'=2] {'tp_0'}, dimensions={0} | all-to-all | bytes 4194304 | tf_op jit(solution)/shard_map/all_to_all | solution.py:109
  212.2 0.4 convert_reduce_fusion
  212.6 0.9 add_convert_fusion
  (191 shorter events, 15.8 us)
Async XLA Ops:
  6.5 109.8 %all-gather.2.cloned.1.call-start = ((), (), s32[]{:S(2)}) async-start(), calls=%async_computation.7 | async-start | bytes 6127616 | tf_op jit(solution)/shard_map/all_gather | solution.py:23
  29.9 20.2 %all-to-all-start = ((bf16[16,129,128]{2,1,0:T(8,128)(2,1)}), bf16[16,129,128]{2,1,0:T(8,128)(2,1)S(1)}, u32[]{:S(2)}, u32[]{:S(2)}) async-start(bf16[16,129,128]{2,1,0:T(8,128)(2,1)} %broadcast_in_dim.48), calls=%async_computation | async-start | bytes 1114112 | tf_op jit(solution)/shard_map/all_to_all | solution.py:32
  50.2 1.5 copy-start.1
  50.2 1.4 copy-start.4
  50.5 13.1 %copy-start = (bf16[128,2048]{1,0:T(8,128)(2,1)S(1)}, bf16[128,2048]{1,0:T(8,128)(2,1)}, u32[]{:S(2)}) copy-start(bf16[128,2048]{1,0:T(8,128)(2,1)} %param.15) | copy-start | bytes 1572868
  63.6 3.0 %copy-start.3 = (f32[2048]{0:T(1024)S(1)}, f32[2048]{0:T(1024)}, u32[]{:S(2)}) copy-start(f32[2048]{0:T(1024)} %param.24) | copy-start | bytes 24580
  96.4 8.3 %copy-start.2 = (bf16[704,128]{1,0:T(8,128)(2,1)S(1)}, bf16[704,128]{1,0:T(8,128)(2,1)}, u32[]{:S(2)}) copy-start(bf16[704,128]{1,0:T(8,128)(2,1)} %param.27) | copy-start | bytes 540676
  106.8 49.7 %all-to-all-start.4 = ((bf16[704,16,128]{2,0,1:T(8,128)(2,1)}), bf16[704,16,128]{2,0,1:T(8,128)(2,1)}, u32[]{:S(2)}, u32[]{:S(2)}) async-start(bf16[704,16,128]{2,0,1:T(8,128)(2,1)} %tile.2), calls=%async_computation.4 | async-start | bytes 5767168 | tf_op jit(solution)/shard_map/all_to_all | solution.py:18
Sparse Core Ops, SparseCore 0:
  9.4 66.9 all-gather.1
